TPU v7x, 32 devices: a whole 2x2x4 slice. The times are simulated.
32 devices in a mesh: ep: 8 (over z, core), tp: 4 (over y, x).
Axes of the slice: x: 2, y: 2, z: 4, core: 2. Of those that a mesh axis runs over, the one named last changes fastest.
Arguments:
- queries: bfloat16 [2048, 4096], P('ep', 'tp'), may hold values from -6 to 6
- keys: bfloat16 [2048, 1024], P('ep', 'tp'), may hold values from -6 to 6
- values: bfloat16 [2048, 1024], P('ep', 'tp'), may hold values from -6 to 6
- query_gain: float32 [64], replicated, may hold values from 1 to 11
- key_gain: float32 [64], replicated, may hold values from 1 to 11
- moe_rows: bfloat16 [2048, 4096], P('ep', 'tp'), may hold values from -14 to 14
- route_ids: int32 [2048, 2], P('ep'), may hold values from 0 to 7, all different within a row; in each aligned block of 256 rows (0 to 255, 256 to 511, ...) at most 96 rows name the same one
- group_weight: float32 [2048], P('ep'), may hold values from 0.2 to 1
- expert_weight: float32 [2048, 2], P('ep'), may hold values from 0.05 to 1
- expert_gate: bfloat16 [8, 4096, 2048], P('ep', None, 'tp'), may hold values from -0.09375 to 0.09375
- expert_up: bfloat16 [8, 4096, 2048], P('ep', None, 'tp'), may hold values from -0.09375 to 0.09375
- expert_down: bfloat16 [8, 2048, 4096], P('ep', None, 'tp'), may hold values from -0.125 to 0.125
Outputs:
- attended: bfloat16 [2048, 4096], P('ep', 'tp')
- moe_out: bfloat16 [2048, 4096], P('ep', 'tp')
Inputs may be any that keep to these rules, and one draw needn't show every extreme that they name: `route_ids`: each row names 2 different experts. Among the rows of one device no expert is named by more than 96 rows, and in every draw some expert is named by exactly 96 of them.
All inputs are finite; a program needn't handle non-finite values.
Results may differ from a plain program's by a relative error of at most 0.0055.
The roundings to bfloat16 on the way count: a program that leaves them out, or rounds other values in their place, can miss the bound.
Values may be sent and summed in bfloat16 or wider, within the bound.
A program may use at most 128 MiB of HBM per device.

v0:
```python
import jax
import jax.numpy as jnp
from jax import lax
from jax.experimental import pallas as pl
from jax.experimental.pallas import tpu as pltpu
from jax.sharding import PartitionSpec as P

D = 4096
HEAD_DIM = 64
GRID_W = 64
TOPK = 2


def rotary_tables(position):
    pair_count = HEAD_DIM // 4
    grid_pos = jnp.stack([position // GRID_W, position % GRID_W], axis=-1).astype(jnp.float32)
    frequency = 10000.0 ** (-jnp.arange(pair_count, dtype=jnp.float32) / pair_count)
    angles = grid_pos[:, :, None] * frequency
    return (jnp.cos(angles), jnp.sin(angles))


def normed_rotated(rows_in, gain, cosine, sine_of):
    row_count, head_count = (rows_in.shape[0], rows_in.shape[1])
    pair_count = HEAD_DIM // 4
    scaled = rows_in * lax.rsqrt(jnp.mean(rows_in * rows_in, axis=-1, keepdims=True) + 1e-06) * gain
    parted = scaled.reshape(row_count, head_count, 2, 2, pair_count)
    first_half, second = (parted[:, :, :, 0, :], parted[:, :, :, 1, :])
    cos_b, sin_b = (cosine[:, None], sine_of[:, None])
    turned = jnp.stack(
        [first_half * cos_b - second * sin_b, second * cos_b + first_half * sin_b], axis=3
    )
    return turned.reshape(row_count, head_count, HEAD_DIM).astype(jnp.bfloat16)


def attend_block(carried, portion, query_rot, kv_width):
    running_max, denominator, summed = carried
    key_count = portion.shape[0]
    head_count = kv_width // HEAD_DIM
    keys_part = portion[:, :kv_width].reshape(key_count, head_count, HEAD_DIM)
    values_part = portion[:, kv_width:].reshape(key_count, head_count, HEAD_DIM)
    scores = jnp.einsum(
        "tkgd,skd->kgts", query_rot, keys_part, preferred_element_type=jnp.float32
    ) * HEAD_DIM ** (-0.5)
    new_max = jnp.max(scores, axis=-1)
    factor = jnp.exp(running_max - new_max)
    weights = jnp.exp(scores - new_max[..., None])
    denominator = denominator * factor + jnp.sum(weights, axis=-1)
    summed = summed * factor[..., None] + jnp.einsum(
        "kgts,skd->kgtd",
        weights.astype(jnp.bfloat16),
        values_part,
        preferred_element_type=jnp.float32,
    )
    return (new_max, denominator, summed)


def plain_on_device(
    queries,
    keys,
    values,
    query_gain,
    key_gain,
    moe_rows,
    route_ids,
    group_weight,
    expert_weight,
    expert_gate,
    expert_up,
    expert_down,
):
    tok_rows = queries.shape[0]
    q_heads = queries.shape[1] // HEAD_DIM
    k_heads = keys.shape[1] // HEAD_DIM
    group_size = q_heads // k_heads
    position = lax.axis_index("ep") * tok_rows + jnp.arange(tok_rows, dtype=jnp.int32)
    cosine, sine_of = rotary_tables(position)
    query_rot = normed_rotated(
        queries.astype(jnp.float32).reshape(tok_rows, q_heads, HEAD_DIM),
        query_gain,
        cosine,
        sine_of,
    )
    query_rot = query_rot.reshape(tok_rows, k_heads, group_size, HEAD_DIM)
    key_rot = normed_rotated(
        keys.astype(jnp.float32).reshape(tok_rows, k_heads, HEAD_DIM), key_gain, cosine, sine_of
    )
    kv_width = k_heads * HEAD_DIM
    joined = jnp.concatenate([key_rot.reshape(tok_rows, kv_width), values], axis=1)
    initial = (
        jnp.full((k_heads, group_size, tok_rows), -jnp.inf, jnp.float32),
        jnp.zeros((k_heads, group_size, tok_rows), jnp.float32),
        jnp.zeros((k_heads, group_size, tok_rows, HEAD_DIM), jnp.float32),
    )
    final_max, denominator, summed = attend_block(
        initial, lax.all_gather(joined, "ep", axis=0, tiled=True), query_rot, kv_width
    )
    attended = (
        (summed / denominator[..., None])
        .transpose(2, 0, 1, 3)
        .reshape(tok_rows, q_heads * HEAD_DIM)
        .astype(jnp.bfloat16)
    )
    moe_tokens = moe_rows.shape[0]
    local_experts = expert_gate.shape[0]
    expert_count = local_experts * lax.axis_size("ep")
    capacity = 3 * moe_tokens * TOPK // (2 * expert_count)
    picks = moe_tokens * TOPK
    route_list = route_ids.reshape(picks)
    one_hot = (route_list[:, None] == jnp.arange(expert_count, dtype=jnp.int32)[None, :]).astype(
        jnp.int32
    )
    rank_of = jnp.sum((jnp.cumsum(one_hot, axis=0) - one_hot) * one_hot, axis=1)
    slot_of = route_list * capacity + rank_of
    owner_of = (
        jnp.full((expert_count * capacity,), moe_tokens, jnp.int32)
        .at[slot_of]
        .set(jnp.arange(picks, dtype=jnp.int32) // TOPK)
    )
    padded = jnp.concatenate([moe_rows, jnp.zeros((1, moe_rows.shape[1]), moe_rows.dtype)], axis=0)
    arrived = lax.all_to_all(
        padded[owner_of].reshape(expert_count, capacity, moe_rows.shape[1]),
        "ep",
        split_axis=0,
        concat_axis=1,
        tiled=True,
    )
    portion = lax.all_gather(arrived, "tp", axis=2, tiled=True)
    widened = portion.astype(jnp.float32)
    gate_act = jnp.einsum("erd,edf->erf", portion, expert_gate, preferred_element_type=jnp.float32)
    up_act = jnp.einsum("erd,edf->erf", portion, expert_up, preferred_element_type=jnp.float32)
    square_sum = jnp.sum(widened * widened, axis=2)
    inv_rms = lax.rsqrt(square_sum / D + 1e-06)[..., None]
    hidden = (jax.nn.silu(gate_act * inv_rms) * (up_act * inv_rms)).astype(jnp.bfloat16)
    out_cols = expert_down.shape[2]
    expert_result = jnp.einsum(
        "erf,efd->erd",
        lax.all_gather(hidden, "tp", axis=2, tiled=True),
        expert_down,
        preferred_element_type=jnp.float32,
    ).astype(jnp.bfloat16)
    returned = lax.all_to_all(expert_result, "ep", split_axis=1, concat_axis=0, tiled=True)
    flat_back = returned.reshape(expert_count * capacity, out_cols)
    picked = flat_back[slot_of].reshape(moe_tokens, TOPK, out_cols).astype(jnp.float32)
    mixing = group_weight[:, None] * expert_weight / jnp.sum(expert_weight, axis=1, keepdims=True)
    moe_out = jnp.sum(mixing[:, :, None] * picked, axis=1).astype(jnp.bfloat16)
    return (attended, moe_out)


MESH = pl.DeviceIdType.MESH


def flip(index, mask, width):
    out = 0
    bit = 1
    while bit < width:
        a, b = (index // bit) % 2, (mask // bit) % 2
        out = out + bit * (a + b - 2 * a * b)
        bit *= 2
    return out


def rope_kernel(q_ref, k_ref, v_ref, qg_ref, kg_ref, cos_ref, sin_ref, qo_ref, kv_ref):
    rows = q_ref.shape[0]
    lane = lax.broadcasted_iota(jnp.int32, (rows, 128), 1)
    one = lax.broadcasted_iota(jnp.int32, (128, 128), 0) // HEAD_DIM
    two = lax.broadcasted_iota(jnp.int32, (128, 128), 1) // HEAD_DIM
    spread = jnp.where(one == two, 1.0 / HEAD_DIM, 0.0).astype(jnp.float32)
    first = lane % 32 < 16
    low = lane < HEAD_DIM
    cosine, sine_of = cos_ref[...], sin_ref[...]

    def turned(x, gain):
        x = x.astype(jnp.float32)
        mean = jnp.dot(
            x * x, spread, preferred_element_type=jnp.float32, precision=lax.Precision.HIGHEST
        )
        y = x * lax.rsqrt(mean + 1e-06) * gain
        partner = jnp.where(first, pltpu.roll(y, 112, 1), pltpu.roll(y, 16, 1))
        return y * cosine + partner * sine_of

    q_slabs = q_ref.shape[1] // 128
    k_slabs = k_ref.shape[1] // 128
    per_kv = q_slabs // (2 * k_slabs)
    for s in range(q_slabs):
        r = turned(q_ref[:, s * 128 : (s + 1) * 128], qg_ref[...])
        r = r.astype(jnp.bfloat16).astype(jnp.float32) * HEAD_DIM ** (-0.5)
        moved = pltpu.roll(r, HEAD_DIM, 1)
        if (s // per_kv) % 2 == 0:
            pair = (jnp.where(low, r, 0.0), jnp.where(low, moved, 0.0))
        else:
            pair = (jnp.where(low, 0.0, moved), jnp.where(low, 0.0, r))
        qo_ref[2 * s] = pair[0].astype(jnp.bfloat16)
        qo_ref[2 * s + 1] = pair[1].astype(jnp.bfloat16)
    for s in range(k_slabs):
        kv_ref[s] = turned(k_ref[:, s * 128 : (s + 1) * 128], kg_ref[...]).astype(jnp.bfloat16)
        kv_ref[k_slabs + s] = v_ref[:, s * 128 : (s + 1) * 128]


def main_kernel(
    ep, picks, kv, q_ref, s0_ref, s1_ref, mix_ref, wg_hbm, wu_hbm, wd_hbm,
    att_ref, moe_ref,
    xg, hid, res, ret, kvall, wg, wu, wd,
    w_sem, d_send, d_recv, x_send, x_recv, xr_send, xr_recv,
    h_send, h_recv, hr_send, hr_recv, r_send, r_recv, k_send, k_recv,
):
    me, tme = lax.axis_index("ep"), lax.axis_index("tp")
    tx, ty = flip(tme, 1, 4), flip(tme, 2, 4)
    sides = (tx, ty)
    cap = picks.shape[1]
    half = cap // 2
    pairs = ep // 2
    width = wg.shape[1]
    chan = picks.shape[2]

    weights = [
        pltpu.make_async_copy(a, b, w_sem.at[n])
        for n, (a, b) in enumerate(((wg_hbm.at[0], wg), (wu_hbm.at[0], wu), (wd_hbm.at[0], wd)))
    ]
    for copy in weights:
        copy.start()
    barrier = pltpu.get_barrier_semaphore()
    for j in range(1, ep):
        pl.semaphore_signal(barrier, inc=1, device_id={"ep": flip(me, j, ep)}, device_id_type=MESH)
    for side in sides:
        pl.semaphore_signal(barrier, inc=1, device_id={"tp": side}, device_id_type=MESH)
    pl.semaphore_wait(barrier, ep + 1)

    def remote(src, dst, send, recv, device):
        return pltpu.make_async_remote_copy(
            src_ref=src, dst_ref=dst, send_sem=send, recv_sem=recv,
            device_id=device, device_id_type=MESH,
        )

    def dispatch(j):
        to = flip(me, j, ep)
        return remote(picks.at[to], xg.at[j, tme], d_send.at[j], d_recv.at[j], {"ep": to})

    def keys_out(j):
        return remote(kv, kvall.at[me], k_send.at[j], k_recv.at[j], {"ep": flip(me, j, ep)})

    def keys_on(j):
        block = flip(me, j - 1, ep)
        return remote(
            kvall.at[block], kvall.at[block], k_send.at[j], k_recv.at[j], {"ep": flip(me, 1, ep)}
        )

    def cross(c, n, src=None):
        src = xg.at[c, tme] if src is None else src
        return remote(src, xg.at[c, tme], x_send.at[c, n], x_recv.at[c, n], {"tp": sides[n]})

    def cross_on(c, n):
        part = xg.at[c, sides[n], pl.ds(n * half, half)]
        return remote(part, part, xr_send.at[c, n], xr_recv.at[c, n], {"tp": sides[1 - n]})

    def wide(i, n):
        return remote(
            hid.at[i, tme], hid.at[i, tme], h_send.at[i, n], h_recv.at[i, n], {"tp": sides[n]}
        )

    def wide_on(i, n):
        part = hid.at[i, sides[n], pl.ds(n * cap, cap)]
        return remote(part, part, hr_send.at[i, n], hr_recv.at[i, n], {"tp": sides[1 - n]})

    def back(i, n):
        c = 2 * i + n
        return remote(
            res.at[i, pl.ds(n * cap, cap)], ret.at[me], r_send.at[c], r_recv.at[c],
            {"ep": flip(me, c, ep)},
        )

    for j in range(1, 4):
        dispatch(j).start()
    for j in range(1, ep):
        if j == 1 or j % 2 == 0:
            keys_out(j).start()
    for j in range(4, ep):
        dispatch(j).start()

    xg[0, tme] = picks[me]
    kvall[me] = kv[...]
    for n in range(2):
        cross(0, n, picks.at[me]).start()

    def enter(c):
        dispatch(c).wait_recv()
        for n in range(2):
            cross(c, n).start()

    def relay(i):
        for d in range(2):
            for n in range(2):
                cross(2 * i + d, n).wait_recv()
                cross_on(2 * i + d, n).start()

    for c in range(1, 4):
        enter(c)
    relay(0)
    for copy in weights:
        copy.wait()

    def first_half(i):
        for d in range(2):
            for n in range(2):
                cross_on(2 * i + d, n).wait_recv()
        gate = jnp.zeros((2 * cap, width), jnp.float32)
        up = jnp.zeros((2 * cap, width), jnp.float32)
        square = jnp.zeros((2 * cap, 1), jnp.float32)
        for a in range(4):
            x = xg[pl.ds(2 * i, 2), a].reshape(2 * cap, chan)
            w = x.astype(jnp.float32)
            square = square + jnp.sum(w * w, axis=1, keepdims=True)
            gate = gate + jnp.dot(
                x, wg[a * chan : (a + 1) * chan, :], preferred_element_type=jnp.float32
            )
            up = up + jnp.dot(
                x, wu[a * chan : (a + 1) * chan, :], preferred_element_type=jnp.float32
            )
        inv = lax.rsqrt(square / D + 1e-06)
        g = gate * inv
        hid[i, tme] = (g / (1.0 + jnp.exp(-g)) * (up * inv)).astype(jnp.bfloat16)
        for n in range(2):
            wide(i, n).start()

    def second_half(i):
        for n in range(2):
            wide_on(i, n).wait_recv()
        total = jnp.zeros((2 * cap, chan), jnp.float32)
        for a in range(4):
            total = total + jnp.dot(
                hid[i, a], wd[a * width : (a + 1) * width, :], preferred_element_type=jnp.float32
            )
        res[i] = total.astype(jnp.bfloat16)

        @pl.when(i > 0)
        def _():
            back(i, 0).start()

        @pl.when(i == 0)
        def _():
            ret[me] = res[0, :cap]

        back(i, 1).start()

    heads = q_ref.shape[0]
    slabs = heads // 2
    k_slabs = kv.shape[0] // 2
    per_kv = slabs // (2 * k_slabs)
    keys_total = ep * kv.shape[1]

    def attend(m, carry):
        pp = m // (2 * per_kv)
        k = kvall[:, pp].reshape(keys_total, 128)
        v = kvall[:, k_slabs + pp].reshape(keys_total, 128)
        outs = []
        for d in range(2):
            s = lax.dot_general(
                q_ref[2 * m + d], k, (((1,), (1,)), ((), ())), preferred_element_type=jnp.float32
            )
            p = jnp.exp(s - jnp.max(s, axis=1, keepdims=True))
            den = jnp.sum(p, axis=1, keepdims=True)
            o = jnp.dot(p.astype(jnp.bfloat16), v, preferred_element_type=jnp.float32)
            outs.append(o / den)
        low = lax.broadcasted_iota(jnp.int32, outs[0].shape, 1) < HEAD_DIM
        even = jnp.where(low, outs[0], pltpu.roll(outs[1], HEAD_DIM, 1))
        odd = jnp.where(low, pltpu.roll(outs[0], HEAD_DIM, 1), outs[1])
        side = ((m // per_kv) % 2).astype(jnp.float32)
        both = jnp.where(side == 0.0, even, odd)
        att_ref[:, pl.ds(pl.multiple_of(m * 128, 128), 128)] = both.astype(jnp.bfloat16)
        return carry

    def keys_relay():
        for j in range(2, ep, 2):
            keys_out(j).wait_recv()
            keys_on(j + 1).start()

    def keys_ready():
        keys_out(1).wait_recv()
        for j in range(2, ep, 2):
            keys_on(j + 1).wait_recv()

    def step(i, carry):
        first_half(i)

        @pl.when(i < pairs - 1)
        def _():
            relay(i + 1)

        @pl.when(i == 0)
        def _():
            keys_relay()

        @pl.when(i == 1)
        def _():
            keys_ready()

        @pl.when(i < pairs - 2)
        def _():
            enter(2 * i + 4)
            enter(2 * i + 5)

        begin = slabs * jnp.maximum(i - 1, 0) * 2 // 5
        begin = jnp.where(i == pairs - 1, slabs - 1, begin)
        end = jnp.where(i == 0, 0, slabs * i * 2 // 5)
        end = jnp.where(i == pairs - 2, slabs - 1, end)
        end = jnp.where(i == pairs - 1, slabs, end)

        def hidden_on():
            for n in range(2):
                wide(i, n).wait_recv()
                wide_on(i, n).start()

        def unit(m, carried):
            attend(m, carried)
            pl.when(m == begin)(hidden_on)
            return carried

        lax.fori_loop(begin, end, unit, 0)
        pl.when(begin == end)(hidden_on)
        second_half(i)
        return carry

    lax.fori_loop(0, pairs, step, 0)

    for c in range(1, ep):
        back(c // 2, c % 2).wait_recv()
    everything = ret[...].reshape(ep * cap, chan)
    mix = mix_ref[...]
    one = jnp.dot(s0_ref[...], everything, preferred_element_type=jnp.float32)
    two = jnp.dot(s1_ref[...], everything, preferred_element_type=jnp.float32)
    moe_ref[...] = (mix[:, 0:1] * one + mix[:, 1:2] * two).astype(jnp.bfloat16)

    for c in range(ep):
        for n in range(2):
            cross(c, n).wait_send()
            cross_on(c, n).wait_send()
        if c > 0:
            dispatch(c).wait_send()
            back(c // 2, c % 2).wait_send()
            keys_out(c).wait_send()
    for i in range(pairs):
        for n in range(2):
            wide(i, n).wait_send()
            wide_on(i, n).wait_send()


def on_device(
    queries, keys, values, query_gain, key_gain, moe_rows, route_ids, group_weight,
    expert_weight, expert_gate, expert_up, expert_down,
):
    ep, tp = lax.axis_size("ep"), lax.axis_size("tp")
    moe_tokens, chan = moe_rows.shape
    cap = 3 * moe_tokens * TOPK // (2 * expert_gate.shape[0] * ep)
    fits = tp == 4 and ep == 8 and cap % 32 == 0 and expert_gate.shape[0] == 1
    if not fits or queries.shape[1] // 128 != 8 or keys.shape[1] // 128 != 2:
        return plain_on_device(
            queries, keys, values, query_gain, key_gain, moe_rows, route_ids, group_weight,
            expert_weight, expert_gate, expert_up, expert_down,
        )
    tok = queries.shape[0]
    position = lax.axis_index("ep") * tok + jnp.arange(tok, dtype=jnp.int32)
    lane = jnp.arange(128, dtype=jnp.int32)
    pair_count = HEAD_DIM // 4
    frequency = 10000.0 ** (-(lane % pair_count).astype(jnp.float32) / pair_count)
    on_rows = (lane // (2 * pair_count)) % 2 == 0
    grid_pos = jnp.where(
        on_rows[None, :], (position // GRID_W)[:, None], (position % GRID_W)[:, None]
    ).astype(jnp.float32)
    angles = grid_pos * frequency[None, :]
    sign = jnp.where((lane // pair_count) % 2 == 0, -1.0, 1.0).astype(jnp.float32)
    heads = queries.shape[1] // HEAD_DIM
    slabs = keys.shape[1] // 128
    q_turned, kv = pl.pallas_call(
        rope_kernel,
        out_shape=(
            jax.ShapeDtypeStruct((heads, tok, 128), jnp.bfloat16),
            jax.ShapeDtypeStruct((2 * slabs, tok, 128), jnp.bfloat16),
        ),
    )(
        queries, keys, values,
        jnp.tile(query_gain, 2)[None, :], jnp.tile(key_gain, 2)[None, :],
        jnp.cos(angles), jnp.sin(angles) * sign[None, :],
    )
    picks_all = moe_tokens * TOPK
    route_list = route_ids.reshape(picks_all)
    one_hot = (route_list[:, None] == jnp.arange(ep, dtype=jnp.int32)[None, :]).astype(jnp.int32)
    rank_of = jnp.sum((jnp.cumsum(one_hot, axis=0) - one_hot) * one_hot, axis=1)
    slot_of = (route_list * cap + rank_of).reshape(moe_tokens, TOPK)
    columns = jnp.arange(ep * cap, dtype=jnp.int32)[None, :]
    picked = [(slot_of[:, n : n + 1] == columns).astype(jnp.bfloat16) for n in range(TOPK)]
    sent = lax.dot_general(
        picked[0] + picked[1], moe_rows, (((0,), (0,)), ((), ())),
        preferred_element_type=jnp.float32,
    ).astype(jnp.bfloat16).reshape(ep, cap, chan)
    mixing = group_weight[:, None] * expert_weight / jnp.sum(expert_weight, axis=1, keepdims=True)
    width = expert_gate.shape[2]
    vmem = pl.BlockSpec(memory_space=pltpu.VMEM)
    hbm = pl.BlockSpec(memory_space=pl.ANY)
    dma = pltpu.SemaphoreType.DMA
    bf = jnp.bfloat16
    attended, moe_out = pl.pallas_call(
        lambda *refs: main_kernel(ep, *refs),
        out_shape=(
            jax.ShapeDtypeStruct(queries.shape, bf),
            jax.ShapeDtypeStruct(moe_rows.shape, bf),
        ),
        in_specs=[vmem] * 6 + [hbm] * 3,
        out_specs=(vmem, vmem),
        scratch_shapes=[
            pltpu.VMEM((ep, tp, cap, chan), bf),
            pltpu.VMEM((ep // 2, tp, 2 * cap, width), bf),
            pltpu.VMEM((ep // 2, 2 * cap, chan), bf),
            pltpu.VMEM((ep, cap, chan), bf),
            pltpu.VMEM((ep, 2 * slabs, tok, 128), bf),
            pltpu.VMEM(expert_gate.shape[1:], bf),
            pltpu.VMEM(expert_up.shape[1:], bf),
            pltpu.VMEM(expert_down.shape[1:], bf),
            dma((3,)), dma((ep,)), dma((ep,)),
            dma((ep, 2)), dma((ep, 2)), dma((ep, 2)), dma((ep, 2)),
            dma((ep // 2, 2)), dma((ep // 2, 2)), dma((ep // 2, 2)), dma((ep // 2, 2)),
            dma((ep,)), dma((ep,)), dma((ep,)), dma((ep,)),
        ],
        compiler_params=pltpu.CompilerParams(
            collective_id=0, has_side_effects=True, vmem_limit_bytes=60 * 1024 * 1024
        ),
    )(sent, kv, q_turned, picked[0], picked[1], mixing, expert_gate, expert_up, expert_down)
    return (attended, moe_out)


def solution(mesh):
    placed = (
        P("ep", "tp"),
        P("ep", "tp"),
        P("ep", "tp"),
        P(),
        P(),
        P("ep", "tp"),
        P("ep", None),
        P("ep"),
        P("ep", None),
        P("ep", None, "tp"),
        P("ep", None, "tp"),
        P("ep", None, "tp"),
    )
    return jax.shard_map(
        on_device,
        mesh=mesh,
        in_specs=placed,
        out_specs=(P("ep", "tp"), P("ep", "tp")),
        check_vma=False,
    )
```

profile of v0, /device:TPU:9, one launch (start us, length us, event | category | flops | bytes accessed | tf_op | source)
XLA Modules:
  0.0 149.7 jit_solution(9070953160071856340)
XLA Ops:
  0.6 0.0 copy-start
  0.7 0.7 tile.4
  1.4 0.7 broadcast_in_dim_tile.6.qg_ref
  2.0 0.7 tile.5
  2.7 0.6 broadcast_in_dim_tile.7.kg_ref
  3.3 0.7 fusion.17
  4.0 0.8 copy.28
  4.8 0.1 eq.79
  5.0 0.1 eq.75
  5.1 1.1 reduce-window.6
  6.3 0.2 slice_reduce_fusion
  6.5 0.1 fusion.7
  6.6 0.1 reduce_sum.21
  6.8 0.1 copy.30
  6.9 0.7 multiply_add_fusion
  7.6 0.1 copy.31
  7.7 0.8 broadcast_divide_fusion.refs_5_
  8.5 1.2 sine_multiply_fusion
  9.7 1.1 fusion
  10.8 3.7 %shard_map.131 = (bf16[16,256,128]{2,1,0:T(8,128)(2,1)}, bf16[4,256,128]{2,1,0:T(8,128)(2,1)}) custom-call(bf16[256,1024]{1,0:T(8,128)(2,1)} %q_ref.1, bf16[256,256]{1,0:T(8,128)(2,1)} %k_ref.1, bf16[256,256]{1,0:T(8,128)(2,1)} %v_ref.1, f32[1,128]{1,0:T(1,128)} %broadcast_in_dim_tile.6.qg_ref, f32[1,128]{1,0:T(1,128)} %broadcast_in_dim_tile.7.kg_ref, ...), custom_call_target="tpu_custom_call" | custom-call | tf_op jit(solution)/shard_map/pallas_call | solution.py:472
  14.4 1.9 %convolution_convert_fusion = bf16[768,1024]{1,0:T(8,128)(2,1)} fusion(bf16[256,1024]{1,0:T(8,128)(2,1)S(1)} %copy-done, s32[256]{0:T(256)S(1)} %bitcast.16, s32[256]{0:T(256)S(1)} %bitcast.14), kind=kOutput, calls=%fused_computation | convolution fusion | flops 405012480 | bytes 2099200 | tf_op jit(solution)/shard_map/dot_general | solution.py:490
  16.4 129.6 %shard_map.132 = (bf16[256,1024]{1,0:T(8,128)(2,1)}, bf16[256,1024]{1,0:T(8,128)(2,1)}) custom-call(bf16[8,96,1024]{2,1,0:T(8,128)(2,1)} %bitcast.12, bf16[4,256,128]{2,1,0:T(8,128)(2,1)} %get-tuple-element.4.refs_1_, bf16[16,256,128]{2,1,0:T(8,128)(2,1)} %get-tuple-element.5.refs_2_, bf16[256,768]{1,0:T(8,128)(2,1)} %get-tuple-element.16.refs_3_, ...), custom_call_target="tpu_custom_call" | custom-call | tf_op jit(solution)/shard_map/pallas_call | solution.py:500
  146.0 1.9 %copy.35 = bf16[256,1024]{1,0:T(8,128)(2,1)} copy(bf16[256,1024]{1,0:T(8,128)(2,1)} %get-tuple-element.20) | data formatting | bytes 1048576
  147.9 1.9 %copy.36 = bf16[256,1024]{1,0:T(8,128)(2,1)} copy(bf16[256,1024]{1,0:T(8,128)(2,1)} %get-tuple-element.21) | data formatting | bytes 1048576
  (8 shorter events, 0.1 us)
Async XLA Ops:
  0.6 13.8 %copy-start = (bf16[256,1024]{1,0:T(8,128)(2,1)S(1)}, bf16[256,1024]{1,0:T(8,128)(2,1)}, u32[]{:S(2)}) copy-start(bf16[256,1024]{1,0:T(8,128)(2,1)} %param.17) | copy-start | bytes 1572868
where the time goes:
time: 150 us
  Pallas kernels  133 us (89%)
  local copies, waits for them, and re-layouts  8.02 us (5%)
  other arithmetic  5.79 us (4%)
  matrix products  1.92 us (1%)
    pallas_call x1, Pallas kernels, on_device(): pl.pallas_call(lambda *refs: main_kernel(ep, *refs), out_shape=(jax.Shape...  130 us
    unnamed x5, local copies, waits for them, and re-layouts  4.55 us
    pallas_call x1, Pallas kernels, on_device(): pl.pallas_call(rope_kernel, out_shape=(jax.ShapeDtypeStruct((heads, tok,...  3.67 us

commit v1 on v0

v1 whole, which is shorter than its diff:
```python
import jax
import jax.numpy as jnp
import numpy as np
from jax import lax
from jax.experimental import pallas as pl
from jax.experimental.pallas import tpu as pltpu
from jax.sharding import PartitionSpec as P

D = 4096
HEAD_DIM = 64
GRID_W = 64
TOPK = 2


def rotary_tables(position):
    pair_count = HEAD_DIM // 4
    grid_pos = jnp.stack([position // GRID_W, position % GRID_W], axis=-1).astype(jnp.float32)
    frequency = 10000.0 ** (-jnp.arange(pair_count, dtype=jnp.float32) / pair_count)
    angles = grid_pos[:, :, None] * frequency
    return (jnp.cos(angles), jnp.sin(angles))


def normed_rotated(rows_in, gain, cosine, sine_of):
    row_count, head_count = (rows_in.shape[0], rows_in.shape[1])
    pair_count = HEAD_DIM // 4
    scaled = rows_in * lax.rsqrt(jnp.mean(rows_in * rows_in, axis=-1, keepdims=True) + 1e-06) * gain
    parted = scaled.reshape(row_count, head_count, 2, 2, pair_count)
    first_half, second = (parted[:, :, :, 0, :], parted[:, :, :, 1, :])
    cos_b, sin_b = (cosine[:, None], sine_of[:, None])
    turned = jnp.stack(
        [first_half * cos_b - second * sin_b, second * cos_b + first_half * sin_b], axis=3
    )
    return turned.reshape(row_count, head_count, HEAD_DIM).astype(jnp.bfloat16)


def attend_block(carried, portion, query_rot, kv_width):
    running_max, denominator, summed = carried
    key_count = portion.shape[0]
    head_count = kv_width // HEAD_DIM
    keys_part = portion[:, :kv_width].reshape(key_count, head_count, HEAD_DIM)
    values_part = portion[:, kv_width:].reshape(key_count, head_count, HEAD_DIM)
    scores = jnp.einsum(
        "tkgd,skd->kgts", query_rot, keys_part, preferred_element_type=jnp.float32
    ) * HEAD_DIM ** (-0.5)
    new_max = jnp.max(scores, axis=-1)
    factor = jnp.exp(running_max - new_max)
    weights = jnp.exp(scores - new_max[..., None])
    denominator = denominator * factor + jnp.sum(weights, axis=-1)
    summed = summed * factor[..., None] + jnp.einsum(
        "kgts,skd->kgtd",
        weights.astype(jnp.bfloat16),
        values_part,
        preferred_element_type=jnp.float32,
    )
    return (new_max, denominator, summed)


def plain_on_device(
    queries,
    keys,
    values,
    query_gain,
    key_gain,
    moe_rows,
    route_ids,
    group_weight,
    expert_weight,
    expert_gate,
    expert_up,
    expert_down,
):
    tok_rows = queries.shape[0]
    q_heads = queries.shape[1] // HEAD_DIM
    k_heads = keys.shape[1] // HEAD_DIM
    group_size = q_heads // k_heads
    position = lax.axis_index("ep") * tok_rows + jnp.arange(tok_rows, dtype=jnp.int32)
    cosine, sine_of = rotary_tables(position)
    query_rot = normed_rotated(
        queries.astype(jnp.float32).reshape(tok_rows, q_heads, HEAD_DIM),
        query_gain,
        cosine,
        sine_of,
    )
    query_rot = query_rot.reshape(tok_rows, k_heads, group_size, HEAD_DIM)
    key_rot = normed_rotated(
        keys.astype(jnp.float32).reshape(tok_rows, k_heads, HEAD_DIM), key_gain, cosine, sine_of
    )
    kv_width = k_heads * HEAD_DIM
    joined = jnp.concatenate([key_rot.reshape(tok_rows, kv_width), values], axis=1)
    initial = (
        jnp.full((k_heads, group_size, tok_rows), -jnp.inf, jnp.float32),
        jnp.zeros((k_heads, group_size, tok_rows), jnp.float32),
        jnp.zeros((k_heads, group_size, tok_rows, HEAD_DIM), jnp.float32),
    )
    final_max, denominator, summed = attend_block(
        initial, lax.all_gather(joined, "ep", axis=0, tiled=True), query_rot, kv_width
    )
    attended = (
        (summed / denominator[..., None])
        .transpose(2, 0, 1, 3)
        .reshape(tok_rows, q_heads * HEAD_DIM)
        .astype(jnp.bfloat16)
    )
    moe_tokens = moe_rows.shape[0]
    local_experts = expert_gate.shape[0]
    expert_count = local_experts * lax.axis_size("ep")
    capacity = 3 * moe_tokens * TOPK // (2 * expert_count)
    picks = moe_tokens * TOPK
    route_list = route_ids.reshape(picks)
    one_hot = (route_list[:, None] == jnp.arange(expert_count, dtype=jnp.int32)[None, :]).astype(
        jnp.int32
    )
    rank_of = jnp.sum((jnp.cumsum(one_hot, axis=0) - one_hot) * one_hot, axis=1)
    slot_of = route_list * capacity + rank_of
    owner_of = (
        jnp.full((expert_count * capacity,), moe_tokens, jnp.int32)
        .at[slot_of]
        .set(jnp.arange(picks, dtype=jnp.int32) // TOPK)
    )
    padded = jnp.concatenate([moe_rows, jnp.zeros((1, moe_rows.shape[1]), moe_rows.dtype)], axis=0)
    arrived = lax.all_to_all(
        padded[owner_of].reshape(expert_count, capacity, moe_rows.shape[1]),
        "ep",
        split_axis=0,
        concat_axis=1,
        tiled=True,
    )
    portion = lax.all_gather(arrived, "tp", axis=2, tiled=True)
    widened = portion.astype(jnp.float32)
    gate_act = jnp.einsum("erd,edf->erf", portion, expert_gate, preferred_element_type=jnp.float32)
    up_act = jnp.einsum("erd,edf->erf", portion, expert_up, preferred_element_type=jnp.float32)
    square_sum = jnp.sum(widened * widened, axis=2)
    inv_rms = lax.rsqrt(square_sum / D + 1e-06)[..., None]
    hidden = (jax.nn.silu(gate_act * inv_rms) * (up_act * inv_rms)).astype(jnp.bfloat16)
    out_cols = expert_down.shape[2]
    expert_result = jnp.einsum(
        "erf,efd->erd",
        lax.all_gather(hidden, "tp", axis=2, tiled=True),
        expert_down,
        preferred_element_type=jnp.float32,
    ).astype(jnp.bfloat16)
    returned = lax.all_to_all(expert_result, "ep", split_axis=1, concat_axis=0, tiled=True)
    flat_back = returned.reshape(expert_count * capacity, out_cols)
    picked = flat_back[slot_of].reshape(moe_tokens, TOPK, out_cols).astype(jnp.float32)
    mixing = group_weight[:, None] * expert_weight / jnp.sum(expert_weight, axis=1, keepdims=True)
    moe_out = jnp.sum(mixing[:, :, None] * picked, axis=1).astype(jnp.bfloat16)
    return (attended, moe_out)


MESH = pl.DeviceIdType.MESH


def flip(index, mask, width):
    out = 0
    bit = 1
    while bit < width:
        a, b = (index // bit) % 2, (mask // bit) % 2
        out = out + bit * (a + b - 2 * a * b)
        bit *= 2
    return out


def sub_iota(shape):
    return lax.broadcasted_iota(jnp.int32, shape, 0)


def lane_iota(shape):
    return lax.broadcasted_iota(jnp.int32, shape, 1)


def main_kernel(
    ep, cap,
    qg_ref, kg_ref, rowtab, coltab, route_ref, gw_ref, ew_ref,
    rows_hbm, k_hbm, v_hbm, q_hbm, wg_hbm, wu_hbm, wd_hbm,
    att_hbm, moe_hbm,
    rows_v, k_v, v_v, q_v, code_ref, pick0, pick1, mix_ref, picks,
    xg, hid, res, ret, kvall, q_s, cos_ref, sin_ref, acc, att_v, moe_v, wg, wu, wd,
    l_sem, o_sem, d_send, d_recv, x_send, x_recv, xr_send, xr_recv,
    h_send, h_recv, hr_send, hr_recv, r_send, r_recv, k_send, k_recv,
):
    me, tme = lax.axis_index("ep"), lax.axis_index("tp")
    sides = (flip(tme, 1, 4), flip(tme, 2, 4))
    half = cap // 2
    width = wg.shape[1]
    tok, chan = rows_v.shape
    f32, bf = jnp.float32, jnp.bfloat16

    def mask(p):
        if isinstance(p, int):
            return 0 if p == 0 else p % (ep - 1) + 1
        return jnp.where(p == 0, 0, p % (ep - 1) + 1)

    def peer(p):
        return flip(me, mask(p), ep)

    pairs = (
        (rows_hbm, rows_v), (k_hbm, k_v), (v_hbm, v_v), (q_hbm, q_v),
        (wg_hbm.at[0], wg), (wu_hbm.at[0], wu), (wd_hbm.at[0], wd),
    )
    loads = [pltpu.make_async_copy(a, b, l_sem.at[n]) for n, (a, b) in enumerate(pairs)]
    for copy in loads:
        copy.start()
    barrier = pltpu.get_barrier_semaphore()
    for j in range(1, ep):
        pl.semaphore_signal(barrier, inc=1, device_id={"ep": flip(me, j, ep)}, device_id_type=MESH)
    for side in sides:
        pl.semaphore_signal(barrier, inc=1, device_id={"tp": side}, device_id_type=MESH)

    def remote(src, dst, send, recv, device):
        return pltpu.make_async_remote_copy(
            src_ref=src, dst_ref=dst, send_sem=send, recv_sem=recv,
            device_id=device, device_id_type=MESH,
        )

    def dispatch(p):
        return remote(picks.at[p], xg.at[p, tme], d_send.at[p], d_recv.at[p], {"ep": peer(p)})

    def keys_out(j):
        return remote(
            kvall.at[me], kvall.at[me], k_send.at[j], k_recv.at[j], {"ep": flip(me, j, ep)}
        )

    def keys_on(j, to):
        block = flip(me, j, ep)
        n = flip(j, to, ep)
        return remote(
            kvall.at[block], kvall.at[block], k_send.at[n], k_recv.at[n],
            {"ep": flip(me, to, ep)},
        )

    def cross(p, n):
        part = xg.at[p, tme]
        return remote(part, part, x_send.at[p, n], x_recv.at[p, n], {"tp": sides[n]})

    def cross_on(p, n):
        part = xg.at[p, sides[n], pl.ds(n * half, half)]
        return remote(part, part, xr_send.at[p, n], xr_recv.at[p, n], {"tp": sides[1 - n]})

    def wide(p, n):
        part = hid.at[p, tme]
        return remote(part, part, h_send.at[p, n], h_recv.at[p, n], {"tp": sides[n]})

    def wide_on(p, n):
        part = hid.at[p, sides[n], pl.ds(n * half, half)]
        return remote(part, part, hr_send.at[p, n], hr_recv.at[p, n], {"tp": sides[1 - n]})

    def back(p):
        return remote(res.at[p], ret.at[p], r_send.at[p], r_recv.at[p], {"ep": peer(p)})

    experts = sub_iota((16, tok))
    first = route_ref[0:1, :] == experts
    second = route_ref[1:2, :] == experts
    both = jnp.logical_or(first, second)
    earlier = jnp.where(sub_iota((tok, tok)) < lane_iota((tok, tok)), 1.0, 0.0).astype(bf)
    rank = jnp.dot(
        jnp.where(both, 1.0, 0.0).astype(bf), earlier, preferred_element_type=f32
    )
    code = jnp.where(both, rank, -1.0)
    for e in range(ep):
        code_ref[e] = code[e : e + 1, :]
    slots = sub_iota((cap, tok)).astype(f32)

    def select(p):
        chosen = jnp.where(code_ref[peer(p)] == slots, 1.0, 0.0).astype(bf)
        return jnp.dot(chosen, rows_v[...], preferred_element_type=f32).astype(bf)

    loads[0].wait()
    xg[0, tme] = select(0)
    picks[1] = select(1)
    pl.semaphore_wait(barrier, ep + 1)
    for n in range(2):
        cross(0, n).start()
    dispatch(1).start()
    for p in range(2, 5):
        picks[p] = select(p)
        dispatch(p).start()

    spread = jnp.where(
        sub_iota((128, 128)) // HEAD_DIM == lane_iota((128, 128)) // HEAD_DIM, 1.0 / HEAD_DIM, 0.0
    ).astype(f32)
    grid_rows = tok // GRID_W
    for g in range(grid_rows):
        line = rowtab[me * grid_rows + g]
        cos_ref[g * GRID_W : (g + 1) * GRID_W, :] = line[:, :128] + coltab[:, :128]
        sin_ref[g * GRID_W : (g + 1) * GRID_W, :] = line[:, 128:] + coltab[:, 128:]
    lane = lane_iota((tok, 128))
    half_one = lane % 32 < 16
    low = lane < HEAD_DIM

    def turned(x, gain):
        x = x.astype(f32)
        mean = jnp.dot(
            x * x, spread, preferred_element_type=f32, precision=lax.Precision.HIGHEST
        )
        y = x * lax.rsqrt(mean + 1e-06) * gain
        partner = jnp.where(half_one, pltpu.roll(y, 112, 1), pltpu.roll(y, 16, 1))
        return y * cos_ref[...] + partner * sin_ref[...]

    q_gain = jnp.concatenate([qg_ref[...], qg_ref[...]], axis=1)
    k_gain = jnp.concatenate([kg_ref[...], kg_ref[...]], axis=1)
    k_slabs = k_v.shape[1] // 128
    slabs = q_v.shape[1] // 128
    per_kv = slabs // (2 * k_slabs)
    loads[1].wait()
    loads[2].wait()
    for s in range(k_slabs):
        kvall[me, s] = turned(k_v[:, s * 128 : (s + 1) * 128], k_gain).astype(bf)
        kvall[me, k_slabs + s] = v_v[:, s * 128 : (s + 1) * 128]
    picks[5] = select(5)
    for j in (1, 2, 4):
        keys_out(j).start()
    for p in range(5, ep):
        if p > 5:
            picks[p] = select(p)
        dispatch(p).start()

    loads[3].wait()
    for s in range(slabs):
        r = turned(q_v[:, s * 128 : (s + 1) * 128], q_gain)
        r = r.astype(bf).astype(f32) * HEAD_DIM ** (-0.5)
        moved = pltpu.roll(r, HEAD_DIM, 1)
        if (s // per_kv) % 2 == 0:
            pair = (jnp.where(low, r, 0.0), jnp.where(low, moved, 0.0))
        else:
            pair = (jnp.where(low, 0.0, moved), jnp.where(low, 0.0, r))
        q_s[2 * s] = pair[0].astype(bf)
        q_s[2 * s + 1] = pair[1].astype(bf)

    columns = lane_iota((16, ep * cap))
    place = jnp.zeros((16, ep * cap), jnp.int32)
    for n in range(1, ep):
        place = place + jnp.where(columns >= n * cap, 1, 0)
    xor_of = jnp.where(place == 0, 0, jnp.where(place == ep - 1, 1, place + 1))
    named = jnp.where(sub_iota((16, ep * cap)) == jnp.bitwise_xor(xor_of, me), 1.0, 0.0).astype(bf)
    rest = (columns - place * cap).astype(f32)[0:1, :]
    for wanted, out in ((first, pick0), (second, pick1)):
        of_token = jnp.where(wanted, rank, -1.0).T.astype(bf)
        spot = jnp.dot(of_token, named, preferred_element_type=f32)
        out[...] = jnp.where(spot == rest, 1.0, 0.0).astype(bf)
    weight = gw_ref[...] * ew_ref[...] / jnp.sum(ew_ref[...], axis=0, keepdims=True)
    mix_ref[...] = jnp.concatenate([weight, jnp.zeros((6, tok), f32)], axis=0).T

    def enter(p):
        dispatch(p).wait_recv()
        for n in range(2):
            cross(p, n).start()

    def relay(p):
        for n in range(2):
            cross(p, n).wait_recv()
            cross_on(p, n).start()

    enter(1)
    relay(0)
    enter(2)
    relay(1)
    for copy in loads[4:]:
        copy.wait()

    def first_half(p):
        for n in range(2):
            cross_on(p, n).wait_recv()
        gate = jnp.zeros((cap, width), f32)
        up = jnp.zeros((cap, width), f32)
        square = jnp.zeros((cap, 1), f32)
        for a in range(4):
            x = xg[p, a]
            w = x.astype(f32)
            square = square + jnp.sum(w * w, axis=1, keepdims=True)
            gate = gate + jnp.dot(x, wg[a * chan : (a + 1) * chan, :], preferred_element_type=f32)
            up = up + jnp.dot(x, wu[a * chan : (a + 1) * chan, :], preferred_element_type=f32)
        inv = lax.rsqrt(square / D + 1e-06)
        g = gate * inv
        hid[p, tme] = (g / (1.0 + jnp.exp(-g)) * (up * inv)).astype(bf)
        for n in range(2):
            wide(p, n).start()

    def second_half(p):
        for n in range(2):
            wide_on(p, n).wait_recv()
        total = jnp.zeros((cap, chan), f32)
        for a in range(4):
            total = total + jnp.dot(
                hid[p, a], wd[a * width : (a + 1) * width, :], preferred_element_type=f32
            )
        return total.astype(bf)

    keys_total = ep * tok

    def attend(m, carry):
        pp = m // (2 * per_kv)
        k = kvall[:, pp].reshape(keys_total, 128)
        v = kvall[:, k_slabs + pp].reshape(keys_total, 128)
        outs = []
        for d in range(2):
            s = lax.dot_general(
                q_s[2 * m + d], k, (((1,), (1,)), ((), ())), preferred_element_type=f32
            )
            p = jnp.exp(s - jnp.max(s, axis=1, keepdims=True))
            den = jnp.sum(p, axis=1, keepdims=True)
            o = jnp.dot(p.astype(bf), v, preferred_element_type=f32)
            outs.append(o / den)
        even = jnp.where(low, outs[0], pltpu.roll(outs[1], HEAD_DIM, 1))
        odd = jnp.where(low, pltpu.roll(outs[0], HEAD_DIM, 1), outs[1])
        side = ((m // per_kv) % 2).astype(f32)
        joined = jnp.where(side == 0.0, even, odd)
        att_v[:, pl.ds(pl.multiple_of(m * 128, 128), 128)] = joined.astype(bf)
        return carry

    def step(i, carry):
        first_half(i)

        @pl.when(i < ep - 3)
        def _():
            enter(i + 3)

        @pl.when(i < ep - 2)
        def _():
            relay(i + 2)

        @pl.when(i == 1)
        def _():
            ret[0] = second_half(0)

        @pl.when(i > 1)
        def _():
            res[i - 1] = second_half(i - 1)
            back(i - 1).start()

        @pl.when(i == KEYS_AT)
        def _():
            keys_out(2).wait_recv()
            keys_on(2, 1).start()
            keys_out(4).wait_recv()
            keys_on(4, 2).start()
            keys_on(4, 1).start()

        @pl.when(i == KEYS_AT + 1)
        def _():
            keys_on(4, 2).wait_recv()
            keys_on(6, 1).start()
            keys_out(1).wait_recv()
            for j in (2, 4, 6):
                keys_on(j, 1).wait_recv()

        begin = jnp.clip((i - UNITS_AT) * UNITS, 0, slabs)
        end = jnp.clip((i - UNITS_AT + 1) * UNITS, 0, slabs)
        lax.fori_loop(begin, end, attend, 0)
        for n in range(2):
            wide(i, n).wait_recv()
            wide_on(i, n).start()
        return carry

    lax.fori_loop(0, ep, step, 0)
    att_out = pltpu.make_async_copy(att_v, att_hbm, o_sem.at[0])
    att_out.start()

    def weighed(start, rows):
        block = ret[start : start + rows].reshape(rows * cap, chan)
        span = slice(start * cap, (start + rows) * cap)
        one = jnp.dot(pick0[:, span], block, preferred_element_type=f32)
        two = jnp.dot(pick1[:, span], block, preferred_element_type=f32)
        return mix_ref[:, 0:1] * one + mix_ref[:, 1:2] * two

    for p in range(1, ep - 2):
        back(p).wait_recv()
    acc[...] = weighed(0, ep - 2)
    res[ep - 1] = second_half(ep - 1)
    back(ep - 1).start()
    back(ep - 2).wait_recv()
    back(ep - 1).wait_recv()
    moe_v[...] = (acc[...] + weighed(ep - 2, 2)).astype(bf)
    moe_out = pltpu.make_async_copy(moe_v, moe_hbm, o_sem.at[1])
    moe_out.start()

    for p in range(ep):
        for n in range(2):
            cross(p, n).wait_send()
            cross_on(p, n).wait_send()
            wide(p, n).wait_send()
            wide_on(p, n).wait_send()
        if p > 0:
            dispatch(p).wait_send()
            back(p).wait_send()
    for j in (1, 2, 4):
        keys_out(j).wait_send()
    keys_on(4, 2).wait_send()
    for j in (2, 4, 6):
        keys_on(j, 1).wait_send()
    att_out.wait()
    moe_out.wait()


KEYS_AT = 2
UNITS_AT = 3
UNITS = 2


def angle_tables(lines):
    lane = np.arange(128)
    pair_count = HEAD_DIM // 4
    frequency = (10000.0 ** (-(lane % pair_count) / pair_count)).astype(np.float32)
    on_rows = (lane // (2 * pair_count)) % 2 == 0
    sign = np.where((lane // pair_count) % 2 == 0, -1.0, 1.0)

    def table(count, mine):
        angle = (np.arange(count, dtype=np.float32)[:, None] * frequency).astype(np.float64)
        both = np.concatenate(
            [np.cos(angle) * mine, np.sin(angle) * sign * mine], axis=1
        )
        return both.astype(np.float32)

    return table(lines, on_rows)[:, None, :], table(GRID_W, ~on_rows)


def on_device(
    queries, keys, values, query_gain, key_gain, moe_rows, route_ids, group_weight,
    expert_weight, expert_gate, expert_up, expert_down,
):
    ep, tp = lax.axis_size("ep"), lax.axis_size("tp")
    moe_tokens, chan = moe_rows.shape
    tok = queries.shape[0]
    cap = 3 * moe_tokens * TOPK // (2 * expert_gate.shape[0] * ep)
    fits = tp == 4 and ep == 8 and cap % 32 == 0 and expert_gate.shape[0] == 1
    fits = fits and tok == moe_tokens and tok % GRID_W == 0
    if not fits or queries.shape[1] // 128 != 8 or keys.shape[1] // 128 != 2:
        return plain_on_device(
            queries, keys, values, query_gain, key_gain, moe_rows, route_ids, group_weight,
            expert_weight, expert_gate, expert_up, expert_down,
        )
    rowtab, coltab = angle_tables(ep * tok // GRID_W)
    heads = queries.shape[1] // HEAD_DIM
    slabs = keys.shape[1] // 128
    width = expert_gate.shape[2]
    vmem = pl.BlockSpec(memory_space=pltpu.VMEM)
    hbm = pl.BlockSpec(memory_space=pl.ANY)
    dma = pltpu.SemaphoreType.DMA
    bf, f32 = jnp.bfloat16, jnp.float32
    attended, moe_out = pl.pallas_call(
        lambda *refs: main_kernel(ep, cap, *refs),
        out_shape=(
            jax.ShapeDtypeStruct(queries.shape, bf),
            jax.ShapeDtypeStruct(moe_rows.shape, bf),
        ),
        in_specs=[vmem] * 7 + [hbm] * 7,
        out_specs=(hbm, hbm),
        scratch_shapes=[
            pltpu.VMEM(moe_rows.shape, bf),
            pltpu.VMEM(keys.shape, bf),
            pltpu.VMEM(values.shape, bf),
            pltpu.VMEM(queries.shape, bf),
            pltpu.VMEM((ep, 1, tok), f32),
            pltpu.VMEM((tok, ep * cap), bf),
            pltpu.VMEM((tok, ep * cap), bf),
            pltpu.VMEM((tok, 8), f32),
            pltpu.VMEM((ep, cap, chan), bf),
            pltpu.VMEM((ep, tp, cap, chan), bf),
            pltpu.VMEM((ep, tp, cap, width), bf),
            pltpu.VMEM((ep, cap, chan), bf),
            pltpu.VMEM((ep, cap, chan), bf),
            pltpu.VMEM((ep, 2 * slabs, tok, 128), bf),
            pltpu.VMEM((heads, tok, 128), bf),
            pltpu.VMEM((tok, 128), f32),
            pltpu.VMEM((tok, 128), f32),
            pltpu.VMEM((tok, chan), f32),
            pltpu.VMEM(queries.shape, bf),
            pltpu.VMEM(moe_rows.shape, bf),
            pltpu.VMEM(expert_gate.shape[1:], bf),
            pltpu.VMEM(expert_up.shape[1:], bf),
            pltpu.VMEM(expert_down.shape[1:], bf),
            dma((7,)), dma((2,)), dma((ep,)), dma((ep,)),
            dma((ep, 2)), dma((ep, 2)), dma((ep, 2)), dma((ep, 2)),
            dma((ep, 2)), dma((ep, 2)), dma((ep, 2)), dma((ep, 2)),
            dma((ep,)), dma((ep,)), dma((ep,)), dma((ep,)),
        ],
        compiler_params=pltpu.CompilerParams(
            collective_id=0, has_side_effects=True, vmem_limit_bytes=60 * 1024 * 1024
        ),
    )(
        query_gain[None, :], key_gain[None, :], jnp.asarray(rowtab), jnp.asarray(coltab),
        route_ids.T, group_weight[None, :], expert_weight.T,
        moe_rows, keys, values, queries, expert_gate, expert_up, expert_down,
    )
    return (attended, moe_out)


def solution(mesh):
    placed = (
        P("ep", "tp"),
        P("ep", "tp"),
        P("ep", "tp"),
        P(),
        P(),
        P("ep", "tp"),
        P("ep", None),
        P("ep"),
        P("ep", None),
        P("ep", None, "tp"),
        P("ep", None, "tp"),
        P("ep", None, "tp"),
    )
    return jax.shard_map(
        on_device,
        mesh=mesh,
        in_specs=placed,
        out_specs=(P("ep", "tp"), P("ep", "tp")),
        check_vma=False,
    )
```

time: 150 us -> 117 us (0.78)
  Pallas kernels: 133 us -> 112 us
  other arithmetic: 5.79 us -> 0 us
  local copies, waits for them, and re-layouts: 8.02 us -> 3.74 us
  matrix products: 1.92 us -> 0 us
    pallas_call x2 -> x1, Pallas kernels: 133 us -> 112 us  [on_device(): pl.pallas_call(lambda *refs: main_kernel(ep, cap, *refs), out_shape=(jax....]
    another operation x5 -> x0, local copies, waits for them, and re-layouts: 2.61 us -> none  [the longest x2 1.37 us: on_device(): jnp.tile(query_gain, 2)[None, :]]
    dot_general x1 -> x0, matrix products: 1.92 us -> none  [on_device(): lax.dot_general(picked[0] + picked[1], moe_rows, (((0,), (0,)), ((), ()))...]
    unnamed x5 -> x2, local copies, waits for them, and re-layouts: 4.55 us -> 3.74 us
where the time goes in v1:
time: 117 us
  Pallas kernels  112 us (96%)
  local copies, waits for them, and re-layouts  3.74 us (3%)
    pallas_call x1, Pallas kernels, on_device(): pl.pallas_call(lambda *refs: main_kernel(ep, cap, *refs), out_shape=(jax....  112 us
    unnamed x2, local copies, waits for them, and re-layouts  3.74 us

profile of v1, /device:TPU:9, one launch (start us, length us, event | category | flops | bytes accessed | tf_op | source)
XLA Modules:
  0.0 116.5 jit_solution(4405773755817601545)
XLA Ops:
  0.6 112.1 %shard_map.149 = (bf16[256,1024]{1,0:T(8,128)(2,1)}, bf16[256,1024]{1,0:T(8,128)(2,1)}) custom-call(f32[1,64]{1,0:T(1,128)} %bitcast.8, f32[1,64]{1,0:T(1,128)} %bitcast.9, f32[32,1,256]{2,1,0:T(1,128)} %constant.4.clone.refs_2_, f32[64,256]{1,0:T(8,128)} %constant.5.clone.refs_3_, s32[2,256]{1,0:T(2,128)} %bitcast.5, f32[1,256]{1,0:T(1,128)} %bitcast.7, ...), custom_call_target="tpu_custom_call" | custom-call | tf_op jit(solution)/shard_map/pallas_call | solution.py:539
  112.8 1.9 %copy.18 = bf16[256,1024]{1,0:T(8,128)(2,1)} copy(bf16[256,1024]{1,0:T(8,128)(2,1)} %get-tuple-element.4) | data formatting | bytes 1048576
  114.6 1.9 %copy.19 = bf16[256,1024]{1,0:T(8,128)(2,1)} copy(bf16[256,1024]{1,0:T(8,128)(2,1)} %get-tuple-element.5) | data formatting | bytes 1048576

commit v2 on v1

--- a/solution.py
+++ b/solution.py
@@ -174,7 +174,7 @@
     rows_hbm, k_hbm, v_hbm, q_hbm, wg_hbm, wu_hbm, wd_hbm,
     att_hbm, moe_hbm,
     rows_v, k_v, v_v, q_v, code_ref, pick0, pick1, mix_ref, picks,
-    xg, hid, res, ret, kvall, q_s, cos_ref, sin_ref, acc, att_v, moe_v, wg, wu, wd,
+    xg, hid, res, ret, kvall, q_s, tops, dens, part_o, cos_ref, sin_ref, acc, att_v, moe_v, wg, wu, wd,
     l_sem, o_sem, d_send, d_recv, x_send, x_recv, xr_send, xr_recv,
     h_send, h_recv, hr_send, hr_recv, r_send, r_recv, k_send, k_recv,
 ):
@@ -184,10 +184,11 @@
     width = wg.shape[1]
     tok, chan = rows_v.shape
     f32, bf = jnp.float32, jnp.bfloat16
+    order = (0, *range(2, ep), 1)
 
     def mask(p):
         if isinstance(p, int):
-            return 0 if p == 0 else p % (ep - 1) + 1
+            return order[p]
         return jnp.where(p == 0, 0, p % (ep - 1) + 1)
 
     def peer(p):
@@ -215,16 +216,20 @@
     def dispatch(p):
         return remote(picks.at[p], xg.at[p, tme], d_send.at[p], d_recv.at[p], {"ep": peer(p)})
 
+    def slot(b):
+        return b // 2 % 2 * (ep // 2) + b // 4 * 2 + b % 2
+
     def keys_out(j):
+        part = kvall.at[slot(me)]
         return remote(
-            kvall.at[me], kvall.at[me], k_send.at[j], k_recv.at[j], {"ep": flip(me, j, ep)}
+            part, part, k_send.at[j], k_recv.at[j], {"ep": flip(me, j, ep)}
         )
 
     def keys_on(j, to):
-        block = flip(me, j, ep)
+        part = kvall.at[slot(flip(me, j, ep))]
         n = flip(j, to, ep)
         return remote(
-            kvall.at[block], kvall.at[block], k_send.at[n], k_recv.at[n],
+            part, part, k_send.at[n], k_recv.at[n],
             {"ep": flip(me, to, ep)},
         )
 
@@ -271,10 +276,20 @@
     for n in range(2):
         cross(0, n).start()
     dispatch(1).start()
-    for p in range(2, 5):
-        picks[p] = select(p)
-        dispatch(p).start()
-
+    picks[ep - 1] = select(ep - 1)
+    dispatch(ep - 1).start()
+
+    def enter(p):
+        dispatch(p).wait_recv()
+        for n in range(2):
+            cross(p, n).start()
+
+    def relay(p):
+        for n in range(2):
+            cross(p, n).wait_recv()
+            cross_on(p, n).start()
+
+    picks[2] = select(2)
     spread = jnp.where(
         sub_iota((128, 128)) // HEAD_DIM == lane_iota((128, 128)) // HEAD_DIM, 1.0 / HEAD_DIM, 0.0
     ).astype(f32)
@@ -304,15 +319,18 @@
     loads[1].wait()
     loads[2].wait()
     for s in range(k_slabs):
-        kvall[me, s] = turned(k_v[:, s * 128 : (s + 1) * 128], k_gain).astype(bf)
-        kvall[me, k_slabs + s] = v_v[:, s * 128 : (s + 1) * 128]
-    picks[5] = select(5)
-    for j in (1, 2, 4):
+        kvall[slot(me), s] = turned(k_v[:, s * 128 : (s + 1) * 128], k_gain).astype(bf)
+        kvall[slot(me), k_slabs + s] = v_v[:, s * 128 : (s + 1) * 128]
+    for j in (1, 4):
         keys_out(j).start()
-    for p in range(5, ep):
-        if p > 5:
-            picks[p] = select(p)
-        dispatch(p).start()
+    enter(ep - 1)
+    for p in range(3, ep - 1):
+        picks[p] = select(p)
+    relay(0)
+    dispatch(2).start()
+    enter(1)
+    relay(ep - 1)
+    dispatch(3).start()
 
     loads[3].wait()
     for s in range(slabs):
@@ -330,7 +348,9 @@
     place = jnp.zeros((16, ep * cap), jnp.int32)
     for n in range(1, ep):
         place = place + jnp.where(columns >= n * cap, 1, 0)
-    xor_of = jnp.where(place == 0, 0, jnp.where(place == ep - 1, 1, place + 1))
+    xor_of = jnp.zeros((16, ep * cap), jnp.int32)
+    for n in range(ep):
+        xor_of = xor_of + jnp.where(place == n, order[n], 0)
     named = jnp.where(sub_iota((16, ep * cap)) == jnp.bitwise_xor(xor_of, me), 1.0, 0.0).astype(bf)
     rest = (columns - place * cap).astype(f32)[0:1, :]
     for wanted, out in ((first, pick0), (second, pick1)):
@@ -340,20 +360,7 @@
     weight = gw_ref[...] * ew_ref[...] / jnp.sum(ew_ref[...], axis=0, keepdims=True)
     mix_ref[...] = jnp.concatenate([weight, jnp.zeros((6, tok), f32)], axis=0).T
 
-    def enter(p):
-        dispatch(p).wait_recv()
-        for n in range(2):
-            cross(p, n).start()
-
-    def relay(p):
-        for n in range(2):
-            cross(p, n).wait_recv()
-            cross_on(p, n).start()
-
-    enter(1)
-    relay(0)
-    enter(2)
-    relay(1)
+    keys_out(2).start()
     for copy in loads[4:]:
         copy.wait()
 
@@ -372,8 +379,6 @@
         inv = lax.rsqrt(square / D + 1e-06)
         g = gate * inv
         hid[p, tme] = (g / (1.0 + jnp.exp(-g)) * (up * inv)).astype(bf)
-        for n in range(2):
-            wide(p, n).start()
 
     def second_half(p):
         for n in range(2):
@@ -387,18 +392,38 @@
 
     keys_total = ep * tok
 
-    def attend(m, carry):
+    part_keys = keys_total // 2
+
+    def scores(m, d, group):
         pp = m // (2 * per_kv)
-        k = kvall[:, pp].reshape(keys_total, 128)
-        v = kvall[:, k_slabs + pp].reshape(keys_total, 128)
+        blocks = pl.ds(group * (ep // 2), ep // 2)
+        k = kvall[blocks, pp].reshape(part_keys, 128)
+        v = kvall[blocks, k_slabs + pp].reshape(part_keys, 128)
+        s = lax.dot_general(
+            q_s[2 * m + d], k, (((1,), (1,)), ((), ())), preferred_element_type=f32
+        )
+        return s, v
+
+    def near(m, carry):
+        for d in range(2):
+            s, v = scores(m, d, me // 2 % 2)
+            top = jnp.max(s, axis=1, keepdims=True)
+            p = jnp.exp(s - top)
+            tops[2 * m + d] = top
+            dens[2 * m + d] = jnp.sum(p, axis=1, keepdims=True)
+            part_o[2 * m + d] = jnp.dot(p.astype(bf), v, preferred_element_type=f32)
+        return carry
+
+    def far(m, carry):
         outs = []
         for d in range(2):
-            s = lax.dot_general(
-                q_s[2 * m + d], k, (((1,), (1,)), ((), ())), preferred_element_type=f32
-            )
-            p = jnp.exp(s - jnp.max(s, axis=1, keepdims=True))
-            den = jnp.sum(p, axis=1, keepdims=True)
-            o = jnp.dot(p.astype(bf), v, preferred_element_type=f32)
+            s, v = scores(m, d, 1 - me // 2 % 2)
+            before = tops[2 * m + d]
+            top = jnp.maximum(before, jnp.max(s, axis=1, keepdims=True))
+            scale = jnp.exp(before - top)
+            p = jnp.exp(s - top)
+            den = dens[2 * m + d] * scale + jnp.sum(p, axis=1, keepdims=True)
+            o = part_o[2 * m + d] * scale + jnp.dot(p.astype(bf), v, preferred_element_type=f32)
             outs.append(o / den)
         even = jnp.where(low, outs[0], pltpu.roll(outs[1], HEAD_DIM, 1))
         odd = jnp.where(low, pltpu.roll(outs[0], HEAD_DIM, 1), outs[1])
@@ -407,16 +432,55 @@
         att_v[:, pl.ds(pl.multiple_of(m * 128, 128), 128)] = joined.astype(bf)
         return carry
 
+    def attend(i, spot):
+        for plan, unit in ((NEAR, near), (FAR, far)):
+            begin, count, total = jnp.int32(0), jnp.int32(0), 0
+            for n, counts in enumerate(plan):
+                for at, units in zip((2, 0, 1), counts):
+                    if at == spot:
+                        begin = begin + jnp.where(i == n, total, 0)
+                        count = count + jnp.where(i == n, units, 0)
+                    total += units
+            lax.fori_loop(begin, begin + count, unit, 0)
+
     def step(i, carry):
+        attend(i, 2)
         first_half(i)
+        for n in range(2):
+            wide(i, n).start()
+
+        @pl.when(i == LAST_AT)
+        def _():
+            for n in range(2):
+                wide(ep - 1, n).start()
+
+        @pl.when(i == EARLY_LAST)
+        def _():
+            first_half(ep - 1)
+
+        @pl.when(i == NEAR_AT)
+        def _():
+            keys_out(1).wait_recv()
+            keys_on(4, 1).wait_recv()
+
+        @pl.when(i == FAR_AT)
+        def _():
+            keys_on(2, 1).wait_recv()
+            keys_on(6, 1).wait_recv()
+
+
+        attend(i, 0)
+        @pl.when(i < ep - 2)
+        def _():
+            relay(i + 1)
 
         @pl.when(i < ep - 3)
         def _():
-            enter(i + 3)
-
-        @pl.when(i < ep - 2)
-        def _():
-            relay(i + 2)
+            enter(i + 2)
+
+        @pl.when(i < ep - 5)
+        def _():
+            dispatch(i + 4).start()
 
         @pl.when(i == 1)
         def _():
@@ -427,31 +491,32 @@
             res[i - 1] = second_half(i - 1)
             back(i - 1).start()
 
-        @pl.when(i == KEYS_AT)
-        def _():
-            keys_out(2).wait_recv()
-            keys_on(2, 1).start()
+        attend(i, 1)
+        for n in range(2):
+            wide(i, n).wait_recv()
+            wide_on(i, n).start()
+
+        @pl.when(i == NEAR_AT - 1)
+        def _():
             keys_out(4).wait_recv()
             keys_on(4, 2).start()
             keys_on(4, 1).start()
 
-        @pl.when(i == KEYS_AT + 1)
-        def _():
+        @pl.when(i == FAR_AT - 1)
+        def _():
+            keys_out(2).wait_recv()
+            keys_on(2, 1).start()
             keys_on(4, 2).wait_recv()
             keys_on(6, 1).start()
-            keys_out(1).wait_recv()
-            for j in (2, 4, 6):
-                keys_on(j, 1).wait_recv()
-
-        begin = jnp.clip((i - UNITS_AT) * UNITS, 0, slabs)
-        end = jnp.clip((i - UNITS_AT + 1) * UNITS, 0, slabs)
-        lax.fori_loop(begin, end, attend, 0)
-        for n in range(2):
-            wide(i, n).wait_recv()
-            wide_on(i, n).start()
+
+        @pl.when(i == LAST_AT)
+        def _():
+            for n in range(2):
+                wide(ep - 1, n).wait_recv()
+                wide_on(ep - 1, n).start()
         return carry
 
-    lax.fori_loop(0, ep, step, 0)
+    lax.fori_loop(0, ep - 1, step, 0)
     att_out = pltpu.make_async_copy(att_v, att_hbm, o_sem.at[0])
     att_out.start()
 
@@ -462,13 +527,17 @@
         two = jnp.dot(pick1[:, span], block, preferred_element_type=f32)
         return mix_ref[:, 0:1] * one + mix_ref[:, 1:2] * two
 
-    for p in range(1, ep - 2):
+    for p in range(1, ep - 3):
         back(p).wait_recv()
-    acc[...] = weighed(0, ep - 2)
+    acc[...] = weighed(0, ep - 3)
     res[ep - 1] = second_half(ep - 1)
     back(ep - 1).start()
+    res[ep - 2] = second_half(ep - 2)
+    back(ep - 2).start()
+    back(ep - 3).wait_recv()
+    acc[...] = acc[...] + weighed(ep - 3, 1)
+    back(ep - 1).wait_recv()
     back(ep - 2).wait_recv()
-    back(ep - 1).wait_recv()
     moe_v[...] = (acc[...] + weighed(ep - 2, 2)).astype(bf)
     moe_out = pltpu.make_async_copy(moe_v, moe_hbm, o_sem.at[1])
     moe_out.start()
@@ -491,9 +560,12 @@
     moe_out.wait()
 
 
-KEYS_AT = 2
-UNITS_AT = 3
-UNITS = 2
+EARLY_LAST = 0
+LAST_AT = 5
+NEAR_AT = 1
+FAR_AT = 3
+NEAR = ((0, 0, 0), (0, 2, 1), (1, 2, 1), (1, 0, 0), (0, 0, 0), (0, 0, 0), (0, 0, 0))
+FAR = ((0, 0, 0), (0, 0, 0), (0, 0, 0), (0, 1, 1), (1, 1, 1), (1, 1, 1), (0, 0, 0))
 
 
 def angle_tables(lines):
@@ -560,6 +632,9 @@
             pltpu.VMEM((ep, cap, chan), bf),
             pltpu.VMEM((ep, 2 * slabs, tok, 128), bf),
             pltpu.VMEM((heads, tok, 128), bf),
+            pltpu.VMEM((heads, tok, 1), f32),
+            pltpu.VMEM((heads, tok, 1), f32),
+            pltpu.VMEM((heads, tok, 128), f32),
             pltpu.VMEM((tok, 128), f32),
             pltpu.VMEM((tok, 128), f32),
             pltpu.VMEM((tok, chan), f32),

time: 117 us -> 105 us (0.90)
  Pallas kernels: 112 us -> 100 us
    pallas_call x1, Pallas kernels: 112 us -> 100 us  [on_device(): pl.pallas_call(lambda *refs: main_kernel(ep, cap, *refs), out_shape=(jax....]
where the time goes in v2:
time: 105 us
  Pallas kernels  100 us (95%)
  local copies, waits for them, and re-layouts  3.74 us (4%)
    pallas_call x1, Pallas kernels, on_device(): pl.pallas_call(lambda *refs: main_kernel(ep, cap, *refs), out_shape=(jax....  100 us
    unnamed x2, local copies, waits for them, and re-layouts  3.74 us

profile of v2, /device:TPU:9, one launch (start us, length us, event | category | flops | bytes accessed | tf_op | source)
XLA Modules:
  0.0 104.5 jit_solution(9750130556550440122)
XLA Ops:
  0.6 100.1 %shard_map.149 = (bf16[256,1024]{1,0:T(8,128)(2,1)}, bf16[256,1024]{1,0:T(8,128)(2,1)}) custom-call(f32[1,64]{1,0:T(1,128)} %bitcast.8, f32[1,64]{1,0:T(1,128)} %bitcast.9, f32[32,1,256]{2,1,0:T(1,128)} %constant.4.clone.refs_2_, f32[64,256]{1,0:T(8,128)} %constant.5.clone.refs_3_, s32[2,256]{1,0:T(2,128)} %bitcast.5, f32[1,256]{1,0:T(1,128)} %bitcast.7, ...), custom_call_target="tpu_custom_call" | custom-call | tf_op jit(solution)/shard_map/pallas_call | solution.py:611
  100.8 1.9 %copy.18 = bf16[256,1024]{1,0:T(8,128)(2,1)} copy(bf16[256,1024]{1,0:T(8,128)(2,1)} %get-tuple-element.4) | data formatting | bytes 1048576
  102.6 1.9 %copy.19 = bf16[256,1024]{1,0:T(8,128)(2,1)} copy(bf16[256,1024]{1,0:T(8,128)(2,1)} %get-tuple-element.5) | data formatting | bytes 1048576

commit v3 on v2

--- a/solution.py
+++ b/solution.py
@@ -454,9 +454,11 @@
             for n in range(2):
                 wide(ep - 1, n).start()
 
-        @pl.when(i == EARLY_LAST)
-        def _():
-            first_half(ep - 1)
+        @pl.when(i == LAST_AT + 1)
+        def _():
+            for n in range(2):
+                wide(ep - 1, n).wait_recv()
+                wide_on(ep - 1, n).start()
 
         @pl.when(i == NEAR_AT)
         def _():
@@ -481,6 +483,10 @@
         @pl.when(i < ep - 5)
         def _():
             dispatch(i + 4).start()
+
+        @pl.when(i == EARLY_LAST)
+        def _():
+            first_half(ep - 1)
 
         @pl.when(i == 1)
         def _():
@@ -509,11 +515,6 @@
             keys_on(4, 2).wait_recv()
             keys_on(6, 1).start()
 
-        @pl.when(i == LAST_AT)
-        def _():
-            for n in range(2):
-                wide(ep - 1, n).wait_recv()
-                wide_on(ep - 1, n).start()
         return carry
 
     lax.fori_loop(0, ep - 1, step, 0)
@@ -560,12 +561,31 @@
     moe_out.wait()
 
 
+def copy_kernel(att_in, moe_in, att_out, moe_out, held, in_sem, out_sem):
+    rows = held.shape[1]
+    parts = []
+    for src, dst in ((att_in, att_out), (moe_in, moe_out)):
+        for at in range(src.shape[0] // rows):
+            span = pl.ds(at * rows, rows)
+            n = len(parts)
+            parts.append((
+                pltpu.make_async_copy(src.at[span], held.at[n], in_sem.at[n]),
+                pltpu.make_async_copy(held.at[n], dst.at[span], out_sem.at[n]),
+            ))
+    for into, _ in parts:
+        into.start()
+    for into, out in parts:
+        into.wait()
+        out.start()
+    for _, out in parts:
+        out.wait()
+
 EARLY_LAST = 0
-LAST_AT = 5
 NEAR_AT = 1
 FAR_AT = 3
 NEAR = ((0, 0, 0), (0, 2, 1), (1, 2, 1), (1, 0, 0), (0, 0, 0), (0, 0, 0), (0, 0, 0))
-FAR = ((0, 0, 0), (0, 0, 0), (0, 0, 0), (0, 1, 1), (1, 1, 1), (1, 1, 1), (0, 0, 0))
+LAST_AT = 5
+FAR = ((0, 0, 0), (0, 0, 0), (0, 0, 0), (0, 2, 1), (1, 2, 1), (0, 1, 0), (0, 0, 0))
 
 
 def angle_tables(lines):
@@ -656,7 +676,16 @@
         route_ids.T, group_weight[None, :], expert_weight.T,
         moe_rows, keys, values, queries, expert_gate, expert_up, expert_down,
     )
-    return (attended, moe_out)
+    return pl.pallas_call(
+        copy_kernel,
+        out_shape=(
+            jax.ShapeDtypeStruct(queries.shape, bf),
+            jax.ShapeDtypeStruct(moe_rows.shape, bf),
+        ),
+        in_specs=[hbm] * 2,
+        out_specs=(hbm, hbm),
+        scratch_shapes=[pltpu.VMEM((4, tok // 2, chan), bf), dma((4,)), dma((4,))],
+    )(attended, moe_out)
 
 
 def solution(mesh):

time: 105 us -> 103 us (0.981)
  local copies, waits for them, and re-layouts: 3.74 us -> 0 us
  Pallas kernels: 100 us -> 102 us
    unnamed x2 -> x0, local copies, waits for them, and re-layouts: 3.74 us -> none
    pallas_call x0 -> x1, Pallas kernels: none -> 1.98 us  [on_device(): pl.pallas_call(copy_kernel, out_shape=(jax.ShapeDtypeStruct(queries.shape...]
where the time goes in v3:
time: 103 us
  Pallas kernels  102 us (99%)
    pallas_call x1, Pallas kernels, on_device(): pl.pallas_call(lambda *refs: main_kernel(ep, cap, *refs), out_shape=(jax....  100 us

profile of v3, /device:TPU:9, one launch (start us, length us, event | category | flops | bytes accessed | tf_op | source)
XLA Modules:
  0.0 102.8 jit_solution(6904131576715256130)
XLA Ops:
  0.6 100.0 %shard_map.149 = (bf16[256,1024]{1,0:T(8,128)(2,1)}, bf16[256,1024]{1,0:T(8,128)(2,1)}) custom-call(f32[1,64]{1,0:T(1,128)} %bitcast.8, f32[1,64]{1,0:T(1,128)} %bitcast.9, f32[32,1,256]{2,1,0:T(1,128)} %constant.4.clone.refs_2_, f32[64,256]{1,0:T(8,128)} %constant.5.clone.refs_3_, s32[2,256]{1,0:T(2,128)} %bitcast.5, f32[1,256]{1,0:T(1,128)} %bitcast.7, ...), custom_call_target="tpu_custom_call" | custom-call | tf_op jit(solution)/shard_map/pallas_call | solution.py:631
  100.6 2.0 %shard_map.150 = (bf16[256,1024]{1,0:T(8,128)(2,1)}, bf16[256,1024]{1,0:T(8,128)(2,1)}) custom-call(bf16[256,1024]{1,0:T(8,128)(2,1)} %get-tuple-element.4.att_in, bf16[256,1024]{1,0:T(8,128)(2,1)} %get-tuple-element.5.moe_in), custom_call_target="tpu_custom_call" | custom-call | tf_op jit(solution)/shard_map/pallas_call | solution.py:679
